TPU v7x, 256 devices: a whole 4x4x8 slice. The times are simulated.
256 devices in a mesh: sp: 32 (over z, x), fs: 4 (over y), tp: 2 (over core).
Axes of the slice: x: 4, y: 4, z: 8, core: 2. Of those that a mesh axis runs over, the one named last changes fastest.
Arguments:
- inputs: bfloat16 [4, 4096, 2048], P('fs', 'sp'), may hold values from -6 to 6
- input_norm_gain: bfloat16 [2048], replicated, may hold values from 0.099609375 to 1.8984375
- receptance_matrix: bfloat16 [2048, 1024], P('fs', 'tp'), may hold values from -0.125 to 0.125
- key_matrix: bfloat16 [2048, 1024], P('fs', 'tp'), may hold values from -0.125 to 0.125
- value_matrix: bfloat16 [2048, 1024], P('fs', 'tp'), may hold values from -0.125 to 0.125
- pooling_input_weight: bfloat16 [2048, 1024], P('fs', 'tp'), may hold values from -0.125 to 0.125
- decay_lower_matrix: bfloat16 [2048, 128], replicated, may hold values from -0.125 to 0.125
- decay_raise_matrix: bfloat16 [2, 64, 1024], P(None, None, 'tp'), may hold values from -1 to 1
- decay_offset_bias: float32 [2, 1024], P(None, 'tp'), may hold values from -13 to -3
- removal_lower_matrix: bfloat16 [2048, 128], replicated, may hold values from -0.125 to 0.125
- removal_raise_matrix: bfloat16 [2, 64, 1024], P(None, None, 'tp'), may hold values from -1 to 1
- removal_rate_bias: float32 [2, 1024], P(None, 'tp'), may hold values from -9 to 1.5
- tempo_scale: float32 [4, 2, 16, 4096], P('fs', None, 'tp', 'sp'), may hold values from 0.3 to 3.2, as said below
- sudden_decay_extra: float32 [4, 2, 16, 4096], P('fs', None, 'tp', 'sp'), may hold values from -2.8 to 0
- head_norm_gain: bfloat16 [1024], P('tp'), may hold values from 0.099609375 to 1.8984375
- group_mixing_weight: bfloat16 [4, 256, 256], P('tp'), may hold values from -0.375 to 0.375
- attention_output_matrix: bfloat16 [2048, 1024], P('fs', 'tp'), may hold values from -0.125 to 0.125
- pooling_output_matrix: bfloat16 [2048, 1024], P('fs', 'tp'), may hold values from -0.125 to 0.125
Outputs:
- mixed_out: bfloat16 [4, 4096, 2048], P('fs', ('sp', 'tp'))
Inputs may be any that keep to these rules, and one draw needn't show every extreme that they name: `tempo_scale`: positive.
All inputs are finite; a program needn't handle non-finite values.
Results may differ from a plain program's by a relative error of at most 0.017.
Values may be sent and summed in bfloat16 or wider, within the bound.
No kernel may reach another device: no remote copies, remote signals or barrier semaphores. Data moves between devices by JAX's collectives and lax.ppermute only.
A program may use at most 128 MiB of HBM per device.

v0:
```python
import jax
import jax.numpy as jnp
from jax import lax
from jax.sharding import Mesh
from jax.sharding import PartitionSpec as P

HEAD = 64
DECAY_RANK = 64
RATE_RANK = 64
POOL_GROUPS = 4
GROUP_WIDTH = 256
SP = ("sp_0", "sp_1")
SP_TP = ("sp_0", "sp_1", "tp")
norm_eps = 1e-06
head_eps = 0.00064
unit_eps = 1e-06
span_len = 32
highest = lax.Precision.HIGHEST


def filled_with(shard, identity):
    return jax.tree.map(
        lambda a, e: jnp.broadcast_to(jnp.asarray(e, a.dtype), a.shape), shard, identity
    )


def prefix_by_axis(shard, axes, combine, identity, reverse):
    before = start = filled_with(shard, identity)
    total = shard
    for axis in reversed(axes):
        peers, here = (lax.axis_size(axis), lax.axis_index(axis))
        pieces = jax.tree.map(
            lambda part, kind: lax.all_gather(part.astype(kind), axis),
            total,
            (jnp.bfloat16, jnp.bfloat16),
        )
        inside, total = (start, start)
        for k in reversed(range(peers)) if reverse else range(peers):
            passed = k > here if reverse else k < here
            total = combine(
                total, jax.tree.map(lambda part, own: part[k].astype(own.dtype), pieces, shard)
            )
            inside = jax.tree.map(lambda new, old: jnp.where(passed, new, old), total, inside)
        before = combine(inside, before)
    return before


def with_halo(cells, sides, width):
    for axis, dim in sides:
        count = lax.axis_size(axis)
        ends = count - 1
        head = lax.slice_in_dim(cells, 0, width, axis=dim)
        tail = lax.slice_in_dim(cells, cells.shape[dim] - width, cells.shape[dim], axis=dim)
        cells = jnp.concatenate(
            [
                lax.ppermute(tail, axis, [(i, (i + 1) % count) for i in range(ends)]),
                cells,
                lax.ppermute(head, axis, [((i + 1) % count, i) for i in range(ends)]),
            ],
            axis=dim,
        )
    return cells


def contract(form, left, right):
    return jnp.einsum(form, left, right, precision=highest)


def matmul(left, right):
    return contract("...ij,...jk->...ik", left, right)


def project(left, weight):
    return jnp.dot(left, weight, preferred_element_type=jnp.float32).astype(jnp.bfloat16)


def against(row_block, weight):
    return lax.dot_general(
        row_block, weight, (((1,), (1,)), ((), ())), preferred_element_type=jnp.float32
    )


def chain_combine(earlier, later):
    return (matmul(earlier[0], later[0]), matmul(earlier[1], later[0]) + later[1])


def unit_inverse(lower):
    result = jnp.eye(lower.shape[-1], dtype=jnp.float32) - lower
    power = lower
    for level in range(4):
        power = matmul(power, power)
        result = result + matmul(result, power)
    return result


def span_terms(logarithm_decay, unit, removal, written, value, recept):
    inner = jnp.cumsum(logarithm_decay, axis=-2)
    last = inner[..., -1:, :]
    ahead = unit * jnp.exp(inner - logarithm_decay)
    shrink = jnp.exp(-inner)
    remove_scaled = removal * shrink
    write_scaled = written * shrink
    query = recept * jnp.exp(inner)
    spots = jnp.arange(span_len)
    strict = spots[:, None] > spots[None, :]
    within = spots[:, None] >= spots[None, :]
    link_remove = jnp.where(strict, contract("...tk,...sk->...ts", ahead, remove_scaled), 0.0)
    link_write = jnp.where(strict, contract("...tk,...sk->...ts", ahead, write_scaled), 0.0)
    read_remove = jnp.where(within, contract("...tk,...sk->...ts", query, remove_scaled), 0.0)
    read_write = jnp.where(within, contract("...tk,...sk->...ts", query, write_scaled), 0.0)
    inverse = unit_inverse(link_remove)
    pull_map = -matmul(inverse, ahead)
    pull_base = -matmul(inverse, matmul(link_write, value))
    tail = jnp.exp(last - inner)
    remove_tail = removal * tail
    write_tail = written * tail
    transfer = jnp.eye(unit.shape[-1], dtype=jnp.float32) * jnp.exp(last) + contract(
        "...sk,...sj->...kj", pull_map, remove_tail
    )
    carried = contract("...sv,...sk->...vk", pull_base, remove_tail) + contract(
        "...sv,...sk->...vk", value, write_tail
    )
    query_eff = query + matmul(read_remove, pull_map)
    local_read = matmul(read_remove, pull_base) + matmul(read_write, value)
    return (query_eff, local_read, transfer, carried)


def shards(
    inputs,
    input_norm_gain,
    receptance_matrix,
    key_matrix,
    value_matrix,
    pooling_input_weight,
    decay_lower_matrix,
    decay_raise_matrix,
    decay_offset_bias,
    removal_lower_matrix,
    removal_raise_matrix,
    removal_rate_bias,
    tempo_scale,
    sudden_decay_extra,
    head_norm_gain,
    group_mixing_weight,
    attention_output_matrix,
    pooling_output_matrix,
):
    recept_full, key_full, value_full, pool_full, attn_full, pool_back = (
        lax.all_gather(receptance_matrix, "fs", axis=0, tiled=True),
        lax.all_gather(key_matrix, "fs", axis=0, tiled=True),
        lax.all_gather(value_matrix, "fs", axis=0, tiled=True),
        lax.all_gather(pooling_input_weight, "fs", axis=0, tiled=True),
        lax.all_gather(attention_output_matrix, "fs", axis=0, tiled=True),
        lax.all_gather(pooling_output_matrix, "fs", axis=0, tiled=True),
    )
    row_block = inputs[0].astype(jnp.float32)
    normed = (
        row_block
        * lax.rsqrt(jnp.mean(row_block * row_block, axis=-1, keepdims=True) + norm_eps)
        * input_norm_gain.astype(jnp.float32)
    ).astype(jnp.bfloat16)
    tokens = normed.shape[0]
    heads = recept_full.shape[1] // HEAD
    blocks = tokens // span_len
    receptance = project(normed, recept_full).astype(jnp.float32).reshape(tokens, heads, HEAD)
    key_rows = project(normed, key_full).astype(jnp.float32).reshape(tokens, heads, HEAD)
    val_rows = project(normed, value_full).astype(jnp.float32).reshape(tokens, heads, HEAD)
    pool_in = project(normed, pool_full)
    decay_act = jnp.tanh(project(normed, decay_lower_matrix).astype(jnp.float32)).astype(
        jnp.bfloat16
    )
    rate_latent = project(normed, removal_lower_matrix)
    unit_keys = key_rows * lax.rsqrt(
        jnp.sum(key_rows * key_rows, axis=-1, keepdims=True) + unit_eps
    )
    decays = []
    removals = []
    writes = []
    for travel_direction in range(2):
        part = decay_act[:, travel_direction * DECAY_RANK : (travel_direction + 1) * DECAY_RANK]
        decay_pre = decay_offset_bias[travel_direction] + jnp.dot(
            part, decay_raise_matrix[travel_direction], preferred_element_type=jnp.float32
        )
        decay_velocity = jnp.exp(-jax.nn.softplus(-decay_pre) - 0.5).reshape(tokens, heads, HEAD)
        decays.append(
            -decay_velocity * tempo_scale[0, travel_direction].T[:, :, None]
            + sudden_decay_extra[0, travel_direction].T[:, :, None]
        )
        latent = rate_latent[:, travel_direction * RATE_RANK : (travel_direction + 1) * RATE_RANK]
        rate = jax.nn.sigmoid(
            removal_rate_bias[travel_direction]
            + jnp.dot(
                latent, removal_raise_matrix[travel_direction], preferred_element_type=jnp.float32
            )
        )
        rate = rate.reshape(tokens, heads, HEAD)
        removals.append(unit_keys * rate)
        writes.append(key_rows * rate)

    def both_ways(forward, backward):
        stacked = jnp.stack([forward, jnp.flip(backward, axis=0)], axis=0)
        return stacked.reshape(2, blocks, span_len, heads, HEAD).transpose(0, 3, 1, 2, 4)

    query_eff, local_read, transfer, carried = span_terms(
        both_ways(decays[0], decays[1]),
        both_ways(unit_keys, unit_keys),
        both_ways(removals[0], removals[1]),
        both_ways(writes[0], writes[1]),
        both_ways(val_rows, val_rows),
        both_ways(receptance, receptance),
    )
    prefix_map, prefix_sum = lax.associative_scan(chain_combine, (transfer, carried), axis=2)
    total_map = prefix_map[:, :, -1]
    total_sum = prefix_sum[:, :, -1]
    identity_map = jnp.broadcast_to(jnp.eye(HEAD, dtype=jnp.float32), total_map.shape[1:])
    empty = jnp.zeros(total_map.shape[1:], jnp.float32)
    ahead_in = prefix_by_axis(
        (total_map[0], total_sum[0]), SP, chain_combine, (identity_map, empty), False
    )
    behind_in = prefix_by_axis(
        (total_map[1], total_sum[1]), SP, chain_combine, (identity_map, empty), True
    )
    incoming = jnp.stack([ahead_in[1], behind_in[1]], axis=0)
    ending = matmul(incoming[:, :, None], prefix_map) + prefix_sum
    starting = jnp.concatenate([incoming[:, :, None], ending[:, :, :-1]], axis=2)
    reads = contract("...tk,...vk->...tv", query_eff, starting) + local_read
    reads = reads.transpose(0, 2, 3, 1, 4).reshape(2, tokens, heads, HEAD)
    readout = reads[0] + jnp.flip(reads[1], axis=0)
    centred = readout - jnp.mean(readout, axis=-1, keepdims=True)
    spread = jnp.mean(centred * centred, axis=-1, keepdims=True)
    attn_out = (centred * lax.rsqrt(spread + head_eps)).reshape(
        tokens, heads * HEAD
    ) * head_norm_gain.astype(jnp.float32)
    attn_out = attn_out.astype(jnp.bfloat16)
    reach = 2 ** (POOL_GROUPS - 1)
    rimmed = with_halo(pool_in, ((SP, 0),), reach).astype(jnp.float32)
    position = lax.axis_index(SP) * tokens + jnp.arange(tokens)
    length = tokens * lax.axis_size(SP)
    running = rimmed
    window_sums = []
    window_counts = []
    for level in range(POOL_GROUPS):
        shift = 2**level
        running = running[:-shift] + running[shift:]
        window_sums.append(running[reach - shift : reach - shift + tokens])
        upper = jnp.minimum(position + shift, length)
        lower = jnp.maximum(position - shift, 0)
        window_counts.append((upper - lower).astype(jnp.float32))
    window_sums = jnp.stack(window_sums, axis=0)
    window_counts = jnp.stack(window_counts, axis=0)
    pool_vals = pool_in.astype(jnp.float32)
    groups_here = pool_in.shape[1] // GROUP_WIDTH
    diffs = []
    for member in range(groups_here):
        group = lax.axis_index("tp") * groups_here + member
        chosen = lax.dynamic_index_in_dim(
            window_sums[:, :, member * GROUP_WIDTH : (member + 1) * GROUP_WIDTH],
            group,
            0,
            keepdims=False,
        )
        count = lax.dynamic_index_in_dim(window_counts, group, 0, keepdims=False)
        diffs.append(
            chosen / count[:, None]
            - pool_vals[:, member * GROUP_WIDTH : (member + 1) * GROUP_WIDTH]
        )
    pool_diff = jnp.concatenate(diffs, axis=1).astype(jnp.bfloat16)
    mixed = [
        jnp.dot(
            pool_diff[:, member * GROUP_WIDTH : (member + 1) * GROUP_WIDTH],
            group_mixing_weight[member],
            preferred_element_type=jnp.float32,
        )
        for member in range(groups_here)
    ]
    pool_out = jnp.concatenate(mixed, axis=1).astype(jnp.bfloat16)
    attn_half, pool_half = (
        lax.all_to_all(attn_out, "tp", split_axis=0, concat_axis=1, tiled=True),
        lax.all_to_all(pool_out, "tp", split_axis=0, concat_axis=1, tiled=True),
    )
    attn_whole, pool_whole = (
        lax.all_gather(attn_full, "tp", axis=1, tiled=True),
        lax.all_gather(pool_back, "tp", axis=1, tiled=True),
    )
    result = against(attn_half, attn_whole) + against(pool_half, pool_whole)
    return result.astype(jnp.bfloat16)[None]


def solution(mesh):
    split = Mesh(
        mesh.devices.reshape(8, 4, mesh.shape["fs"], mesh.shape["tp"]), ("sp_0", "sp_1", "fs", "tp")
    )
    in_specs = (
        P("fs", SP, None),
        P(),
        P("fs", "tp"),
        P("fs", "tp"),
        P("fs", "tp"),
        P("fs", "tp"),
        P(),
        P(None, None, "tp"),
        P(None, "tp"),
        P(),
        P(None, None, "tp"),
        P(None, "tp"),
        P("fs", None, "tp", SP),
        P("fs", None, "tp", SP),
        P("tp"),
        P("tp", None, None),
        P("fs", "tp"),
        P("fs", "tp"),
    )
    out_specs = P("fs", SP_TP, None)
    return jax.shard_map(
        shards, mesh=split, in_specs=in_specs, out_specs=out_specs, check_vma=False
    )
```

profile of v0, /device:TPU:7, one launch (start us, length us, event | category | flops | bytes accessed | tf_op | source)
XLA Modules:
  0.0 448.1 jit_solution(15655499817770157762)
XLA Ops:
  18.1 27.2 %all-gather.19.cloned.1.call-done = bf16[2048,512]{1,0:T(8,128)(2,1)} async-done(((bf16[512,512]{1,0:T(8,128)(2,1)}), bf16[2048,512]{1,0:T(8,128)(2,1)}) %all-gather.19.cloned.1.call-update) | async-done | bytes 2097168 | tf_op jit(solution)/shard_map/all_gather | solution.py:150
  45.3 2.1 fusion.29
  47.6 32.9 %all-gather.21.cloned.1.call-done = bf16[2048,512]{1,0:T(8,128)(2,1)} async-done(((bf16[512,512]{1,0:T(8,128)(2,1)}), bf16[2048,512]{1,0:T(8,128)(2,1)}) %all-gather.21.cloned.1.call-update) | async-done | bytes 2097168 | tf_op jit(solution)/shard_map/all_gather | solution.py:151
  80.5 2.1 fusion.28
  90.6 3.0 fusion.55
  93.6 3.0 convolution_select_fusion.2
  96.6 1.2 fusion.215
  97.8 1.2 fusion.216
  99.0 1.3 convolution_add_fusion.5
  100.3 1.2 fusion.217
  101.5 1.4 convolution_add_fusion.4
  102.9 2.2 fusion.218
  105.1 2.2 convolution_add_fusion.3
  107.3 4.0 convolution_select_fusion.1
  113.4 1.1 copy.129
  114.5 3.2 convolution_add_fusion.2
  117.8 1.8 convolution_negate_fusion.1
  119.6 1.2 fusion.61
  120.8 1.2 convolution_negate_fusion
  122.0 4.2 fusion.46
  126.3 5.0 %multiply_add_fusion = f32[2,8,4,64,64]{4,3,2,1,0:T(8,128)S(1)} fusion(f32[2,8,4,32,64]{4,3,2,1,0:T(8,128)S(1)} %convolution_negate_fusion.1, f32[2,8,4,64]{3,2,1,0:T(4,128)S(1)} %copy-done.59, f32[64,64]{1,0:T(8,128)S(1)} %fusion.167, f32[2,8,4,32,64]{4,1,2,3,0:T(8,128)} %copy-done.15), kind=kOutput, calls=%fused_computation.8 | convolution fusion | flops 101187584 | bytes 2129920 | tf_op jit(solution)/shard_map/...sk,...sj->...kj/dot_general | solution.py:66
  131.3 1.2 fusion.41
  133.3 4.0 convolution_add_fusion.1
  137.3 1.2 convolution_add_fusion.7
  139.2 1.2 pad_add_fusion
  140.4 1.5 fusion.13
  142.6 1.5 convolution_bitcast_fusion.3
  145.7 11.3 %pad.33 = f32[2,8,4,64,64]{4,3,2,1,0:T(8,128)} pad(f32[2,8,2,64,64]{4,3,2,1,0:T(8,128)S(1)} %copy-done.30, f32[]{:T(128)} %constant.27.clone.1), padding=0_0_0x0_0_0x1_0_1x0_0_0x0_0_0 | pad | bytes 1572868 | tf_op jit(solution)/shard_map/pad | solution.py:212
  157.1 11.2 %pad.32 = f32[2,8,4,64,64]{4,3,2,1,0:T(8,128)} pad(f32[2,8,2,64,64]{4,3,2,1,0:T(8,128)S(1)} %pad_maximum_fusion.1, f32[]{:T(128)} %constant.27.clone.1), padding=0_0_0x0_0_0x0_1_1x0_0_0x0_0_0 | pad | bytes 1572868 | tf_op jit(solution)/shard_map/pad | solution.py:212
  168.3 11.2 %pad.28 = f32[2,8,4,64,64]{4,3,2,1,0:T(8,128)} pad(f32[2,8,2,64,64]{4,3,2,1,0:T(8,128)S(1)} %pad_maximum_fusion, f32[]{:T(128)} %constant.27.clone.1), padding=0_0_0x0_0_0x0_1_1x0_0_0x0_0_0 | pad | bytes 1572868 | tf_op jit(solution)/shard_map/pad | solution.py:212
  179.6 16.7 %pad.29 = f32[2,8,4,64,64]{4,3,2,1,0:T(8,128)} pad(f32[2,8,2,64,64]{4,3,2,1,0:T(8,128)} %pad_add_fusion.1, f32[]{:T(128)} %constant.27.clone.1), padding=0_0_0x0_0_0x1_0_1x0_0_0x0_0_0 | pad | bytes 1572868 | tf_op jit(solution)/shard_map/pad | solution.py:212
  196.3 2.2 add_convert_fusion
  198.5 10.7 %all-gather.6 = bf16[4,8,1,64,64]{4,3,2,1,0:T(8,128)(2,1)S(1)} all-gather(bf16[1,8,1,64,64]{4,3,2,1,0:T(8,128)(2,1)S(1)} %get-tuple-element.24), channel_id=8, replica_groups=mesh['sp_0'=8,'sp_1'=4,'fs'=4,'tp'=2] {'sp_1'}, dimensions={0}, use_global_device_ids=true | all-gather | bytes 327680 | tf_op jit(solution)/shard_map/all_gather | solution.py:33
  209.2 1.9 fusion.200
  211.1 11.9 %all-gather.4 = bf16[4,8,1,64,64]{4,3,2,1,0:T(8,128)(2,1)S(1)} all-gather(bf16[1,8,1,64,64]{4,3,2,1,0:T(8,128)(2,1)S(1)} %get-tuple-element.22), channel_id=6, replica_groups=mesh['sp_0'=8,'sp_1'=4,'fs'=4,'tp'=2] {'sp_1'}, dimensions={0}, use_global_device_ids=true | all-gather | bytes 327680 | tf_op jit(solution)/shard_map/all_gather | solution.py:33
  225.7 22.8 %all-gather.7 = bf16[64,64,64]{2,1,0:T(8,128)(2,1)S(1)} all-gather(bf16[8,64,64]{2,1,0:T(8,128)(2,1)S(1)} %get-tuple-element.46), channel_id=9, replica_groups=mesh['sp_0'=8,'sp_1'=4,'fs'=4,'tp'=2] {'sp_0'}, dimensions={0}, use_global_device_ids=true | all-gather | bytes 589824 | tf_op jit(solution)/shard_map/all_gather | solution.py:33
  249.3 22.2 %all-gather.5 = bf16[64,64,64]{2,1,0:T(8,128)(2,1)S(1)} all-gather(bf16[8,64,64]{2,1,0:T(8,128)(2,1)S(1)} %get-tuple-element.48), channel_id=7, replica_groups=mesh['sp_0'=8,'sp_1'=4,'fs'=4,'tp'=2] {'sp_0'}, dimensions={0}, use_global_device_ids=true | all-gather | bytes 589824 | tf_op jit(solution)/shard_map/all_gather | solution.py:33
  273.1 10.5 %all-gather.2 = bf16[4,8,1,64,64]{4,3,2,1,0:T(8,128)(2,1)S(1)} all-gather(bf16[1,8,1,64,64]{4,3,2,1,0:T(8,128)(2,1)S(1)} %get-tuple-element.23), channel_id=4, replica_groups=mesh['sp_0'=8,'sp_1'=4,'fs'=4,'tp'=2] {'sp_1'}, dimensions={0}, use_global_device_ids=true | all-gather | bytes 327680 | tf_op jit(solution)/shard_map/all_gather | solution.py:33
  283.6 10.3 %all-gather = bf16[4,8,1,64,64]{4,3,2,1,0:T(8,128)(2,1)S(1)} all-gather(bf16[1,8,1,64,64]{4,3,2,1,0:T(8,128)(2,1)S(1)} %get-tuple-element.21), channel_id=2, replica_groups=mesh['sp_0'=8,'sp_1'=4,'fs'=4,'tp'=2] {'sp_1'}, dimensions={0}, use_global_device_ids=true | all-gather | bytes 327680 | tf_op jit(solution)/shard_map/all_gather | solution.py:33
  295.9 20.4 %all-gather.3 = bf16[64,64,64]{2,1,0:T(8,128)(2,1)S(1)} all-gather(bf16[8,64,64]{2,1,0:T(8,128)(2,1)S(1)} %get-tuple-element.50), channel_id=5, replica_groups=mesh['sp_0'=8,'sp_1'=4,'fs'=4,'tp'=2] {'sp_0'}, dimensions={0}, use_global_device_ids=true | all-gather | bytes 589824 | tf_op jit(solution)/shard_map/all_gather | solution.py:33
  317.2 21.5 %all-gather.1 = bf16[64,64,64]{2,1,0:T(8,128)(2,1)S(1)} all-gather(bf16[8,64,64]{2,1,0:T(8,128)(2,1)S(1)} %get-tuple-element.52), channel_id=3, replica_groups=mesh['sp_0'=8,'sp_1'=4,'fs'=4,'tp'=2] {'sp_0'}, dimensions={0}, use_global_device_ids=true | all-gather | bytes 589824 | tf_op jit(solution)/shard_map/all_gather | solution.py:33
  345.2 3.0 fusion.30
  348.6 2.1 fusion.14
  350.7 1.8 copy.91
  352.5 1.9 stack.75
  354.4 1.8 rev.22
  356.2 2.0 copy.92
  358.2 1.3 copy.94
  359.5 1.2 copy.93
  360.8 1.3 fusion.17
  363.4 3.1 convolution_select_fusion.3
  366.5 1.2 fusion.221
  367.7 3.1 convolution_select_fusion
  370.8 1.2 convolution_add_fusion.6
  372.1 2.0 convolution_add_fusion.8
  374.1 2.0 convolution_bitcast_fusion
  376.6 3.4 fusion.9
  382.4 2.1 fusion.214
  384.5 1.9 collective-permute-start.1
  386.4 5.5 %collective-permute-start = (bf16[8,512]{1,0:T(8,128)(2,1)S(1)}, bf16[8,512]{1,0:T(8,128)(2,1)S(1)}, u32[]{:S(2)}, u32[]{:S(2)}) collective-permute-start(bf16[8,512]{1,0:T(8,128)(2,1)S(1)} %get-tuple-element.34), channel_id=1, source_target_pairs={{0,8},{8,16},{16,24},{24,32},{32,40},{40,48},{48,56},{56,64},{64,7... | collective-permute-start | bytes 24584 | tf_op jit(solution)/shard_map/ppermute | solution.py:56
  391.9 35.5 %all_to_all.32 = bf16[2,64,512]{2,1,0:T(8,128)(2,1)S(1)} all-to-all(bf16[2,64,512]{2,1,0:T(8,128)(2,1)S(1)} %multiply_convert_fusion), channel_id=1, replica_groups=mesh['sp_0'=8,'sp_1'=4,'fs'=4,'tp'=2] {'tp'}, dimensions={0} | all-to-all | bytes 262144 | tf_op jit(solution)/shard_map/all_to_all | solution.py:278
  429.2 3.9 all_to_all.33
  433.1 3.6 fusion.222
  436.7 4.3 fusion.1
  (306 shorter events, 45.8 us)
Async XLA Ops:
  6.5 5.0 %copy-start = (bf16[2048,128]{1,0:T(8,128)(2,1)S(1)}, bf16[2048,128]{1,0:T(8,128)(2,1)}, u32[]{:S(2)}) copy-start(bf16[2048,128]{1,0:T(8,128)(2,1)} %param.24) | copy-start | bytes 1572868
  6.5 4.7 %copy-start.68 = (f32[2,512]{1,0:T(2,128)S(1)}, f32[2,512]{1,0:T(2,128)}, u32[]{:S(2)}) copy-start(f32[2,512]{1,0:T(2,128)} %param.26) | copy-start | bytes 12292
  6.5 4.7 %copy-start.67 = (bf16[2048]{0:T(1024)(128)(2,1)S(1)}, bf16[2048]{0:T(1024)(128)(2,1)}, u32[]{:S(2)}) copy-start(bf16[2048]{0:T(1024)(128)(2,1)} %param.19) | copy-start | bytes 12292
  6.5 4.7 %copy-start.5 = (bf16[1,128,2048]{2,1,0:T(8,128)(2,1)S(1)}, bf16[1,128,2048]{2,1,0:T(8,128)(2,1)}, u32[]{:S(2)}) copy-start(bf16[1,128,2048]{2,1,0:T(8,128)(2,1)} %param.18) | copy-start | bytes 1572868
  6.5 38.7 %all-gather.19.cloned.1.call-start = ((), (), s32[]{:S(2)}) async-start(), calls=%async_computation.3 | async-start | bytes 2621440 | tf_op jit(solution)/shard_map/all_gather | solution.py:150
  7.3 73.2 %all-gather.21.cloned.1.call-start = ((), (), s32[]{:S(2)}) async-start(), calls=%async_computation.4 | async-start | bytes 2621440 | tf_op jit(solution)/shard_map/all_gather | solution.py:151
  8.0 3.9 copy-start.74
  8.0 337.1 %all-gather.17.cloned.1.call-start = ((), (), s32[]{:S(2)}) async-start(), calls=%async_computation.2 | async-start | bytes 2621440 | tf_op jit(solution)/shard_map/all_gather | solution.py:149
  8.8 339.4 %all-gather.23.cloned.1.call-start = ((), (), s32[]{:S(2)}) async-start(), calls=%async_computation.5 | async-start | bytes 2621440 | tf_op jit(solution)/shard_map/all_gather | solution.py:153
  9.3 372.0 %all-gather.29.cloned.1.call-start = ((), (), s32[]{:S(2)}) async-start(), calls=%async_computation.8 | async-start | bytes 2621440 | tf_op jit(solution)/shard_map/all_gather | solution.py:154
  9.9 2.6 copy-start.65
  9.9 2.6 copy-start.66
  10.0 372.0 %all-gather.27.cloned.1.call-start = ((), (), s32[]{:S(2)}) async-start(), calls=%async_computation.7 | async-start | bytes 2621440 | tf_op jit(solution)/shard_map/all_gather | solution.py:152
  10.5 422.6 %all-gather.25.cloned.1.call-start = ((), (), s32[]{:S(2)}) async-start(), calls=%async_computation.6 | async-start | bytes 6291456 | tf_op jit(solution)/shard_map/all_gather | solution.py:282
  11.5 69.0 %copy-start.62 = (f32[128]{0:T(128)}, f32[128]{0:T(128)S(1)}, u32[]{:S(2)}) copy-start(f32[128]{0:T(128)S(1)} %add_rsqrt_fusion.2) | copy-start | bytes 1540
  15.0 1.9 copy-start.72
  93.6 4.2 copy-start.9
  93.6 13.7 %copy-start.7 = (f32[2,8,4,32,64]{4,1,2,3,0:T(8,128)}, f32[2,8,4,32,64]{4,1,2,3,0:T(8,128)S(1)}, u32[]{:S(2)}) copy-start(f32[2,8,4,32,64]{4,1,2,3,0:T(8,128)S(1)} %get-tuple-element.12) | copy-start | bytes 1572868
  93.6 28.4 %copy-start.15 = (f32[2,8,4,32,64]{4,1,2,3,0:T(8,128)}, f32[2,8,4,32,64]{4,1,2,3,0:T(8,128)S(1)}, u32[]{:S(2)}) copy-start(f32[2,8,4,32,64]{4,1,2,3,0:T(8,128)S(1)} %get-tuple-element.16) | copy-start | bytes 1572868
  114.5 17.9 %copy-start.22 = (f32[1,4,32,8,64]{4,2,1,3,0:T(8,128)}, f32[1,4,32,8,64]{4,2,1,3,0:T(8,128)S(1)}, u32[]{:S(2)}) copy-start(f32[1,4,32,8,64]{4,2,1,3,0:T(8,128)S(1)} %copy.129) | copy-start | bytes 786436
  117.8 1.8 copy-start.20
  119.6 6.7 %copy-start.11 = (f32[2,8,4,32,64]{4,3,2,1,0:T(8,128)}, f32[2,8,4,32,64]{4,3,2,1,0:T(8,128)S(1)}, u32[]{:S(2)}) copy-start(f32[2,8,4,32,64]{4,3,2,1,0:T(8,128)S(1)} %convolution_negate_fusion.1) | copy-start | bytes 1572868
  122.0 4.3 copy-start.13
  122.0 4.3 copy-start.59
  131.3 11.3 %copy-start.2 = (f32[2,8,4,64,64]{4,3,2,1,0:T(8,128)}, f32[2,8,4,64,64]{4,3,2,1,0:T(8,128)S(1)}, u32[]{:S(2)}) copy-start(f32[2,8,4,64,64]{4,3,2,1,0:T(8,128)S(1)} %multiply_add_fusion) | copy-start | bytes 3145732
  131.3 2.0 copy-start.29
  137.3 4.6 %copy-start.16 = (f32[2,8,4,64,64]{4,3,2,1,0:T(8,128)}, f32[2,8,4,64,64]{4,3,2,1,0:T(8,128)S(1)}, u32[]{:S(2)}) copy-start(f32[2,8,4,64,64]{4,3,2,1,0:T(8,128)S(1)} %convolution_add_fusion.1) | copy-start | bytes 3145732
  145.6 11.3 %slice-start.1 = ((f32[2,8,4,64,64]{4,3,2,1,0:T(8,128)}), f32[2,8,1,64,64]{4,3,2,1,0:T(8,128)S(1)}, s32[]{:S(2)}) async-start(f32[2,8,4,64,64]{4,3,2,1,0:T(8,128)} %copy-done.16), calls=%async_computation.11 | async-start | bytes 1048576 | tf_op jit(solution)/shard_map/slice | solution.py:212
  145.7 11.3 %copy-start.53 = (f32[2,8,1,64,64]{4,3,2,1,0:T(8,128)S(1)}, f32[2,8,1,64,64]{4,3,2,1,0:T(8,128)}, u32[]{:S(2)}) copy-start(f32[2,8,1,64,64]{4,3,2,1,0:T(8,128)} %fusion.13) | copy-start | bytes 786436
  157.0 11.2 %slice-start = ((f32[2,8,4,64,64]{4,3,2,1,0:T(8,128)}), f32[2,8,1,64,64]{4,3,2,1,0:T(8,128)S(1)}, s32[]{:S(2)}) async-start(f32[2,8,4,64,64]{4,3,2,1,0:T(8,128)} %copy-done.2), calls=%async_computation.10 | async-start | bytes 1048576 | tf_op jit(solution)/shard_map/slice | solution.py:212
  157.0 11.2 %copy-start.54 = (f32[2,8,1,64,64]{4,3,2,1,0:T(8,128)S(1)}, f32[2,8,1,64,64]{4,3,2,1,0:T(8,128)}, u32[]{:S(2)}) copy-start(f32[2,8,1,64,64]{4,3,2,1,0:T(8,128)} %convolution_bitcast_fusion.3) | copy-start | bytes 786436
  179.6 16.7 %copy-start.3 = (f32[2,8,4,64,64]{4,3,2,1,0:T(8,128)S(1)}, f32[2,8,4,64,64]{4,3,2,1,0:T(8,128)}, u32[]{:S(2)}) copy-start(f32[2,8,4,64,64]{4,3,2,1,0:T(8,128)} %pad.33) | copy-start | bytes 3145732
  196.3 12.9 %copy-start.18 = (f32[2,8,4,64,64]{4,3,2,1,0:T(8,128)S(1)}, f32[2,8,4,64,64]{4,3,2,1,0:T(8,128)}, u32[]{:S(2)}) copy-start(f32[2,8,4,64,64]{4,3,2,1,0:T(8,128)} %pad.28) | copy-start | bytes 3145732
  196.3 12.9 %copy-start.19 = (f32[2,8,4,64,64]{4,3,2,1,0:T(8,128)S(1)}, f32[2,8,4,64,64]{4,3,2,1,0:T(8,128)}, u32[]{:S(2)}) copy-start(f32[2,8,4,64,64]{4,3,2,1,0:T(8,128)} %pad.29) | copy-start | bytes 3145732
  224.5 24.6 %copy-start.33 = (f32[8,64,64]{2,1,0:T(8,128)}, f32[8,64,64]{2,1,0:T(8,128)S(1)}, u32[]{:S(2)}) copy-start(f32[8,64,64]{2,1,0:T(8,128)S(1)} %convolution_add_fusion.19) | copy-start | bytes 393220
  224.8 24.6 %copy-start.34 = (f32[8,64,64]{2,1,0:T(8,128)}, f32[8,64,64]{2,1,0:T(8,128)S(1)}, u32[]{:S(2)}) copy-start(f32[8,64,64]{2,1,0:T(8,128)S(1)} %convolution_add_fusion.18) | copy-start | bytes 393220
  294.4 22.3 %copy-start.45 = (f32[8,64,64]{2,1,0:T(8,128)}, f32[8,64,64]{2,1,0:T(8,128)S(1)}, u32[]{:S(2)}) copy-start(f32[8,64,64]{2,1,0:T(8,128)S(1)} %convolution_add_fusion.33) | copy-start | bytes 393220
  316.4 24.8 %copy-start.26 = (bf16[64,64,64]{2,1,0:T(8,128)(2,1)}, bf16[64,64,64]{2,1,0:T(8,128)(2,1)S(1)}, u32[]{:S(2)}) copy-start(bf16[64,64,64]{2,1,0:T(8,128)(2,1)S(1)} %all-gather.3) | copy-start | bytes 1572868
  338.7 2.5 copy-start.27
  340.1 2.1 copy-start.35
  340.4 1.8 copy-start.37
  342.6 2.5 copy-start.63
  348.2 88.5 %all-gather.31.cloned.1.call-start = ((), (), s32[]{:S(2)}) async-start(), calls=%async_computation.9 | async-start | bytes 6291456 | tf_op jit(solution)/shard_map/all_gather | solution.py:283
  358.1 2.6 copy-start.36
  358.1 2.6 copy-start.38
  358.1 2.6 copy-start.40
  358.1 2.6 copy-start.42
  358.2 2.6 copy-start.44
  358.2 2.6 copy-start.49
  358.2 2.6 copy-start.56
  358.2 4.0 copy-start.57
  359.5 3.1 copy-start.32
  359.5 3.1 copy-start.46
  359.5 3.1 copy-start.55
  360.8 2.2 copy-start.50
  363.4 3.1 copy-start.14
  367.7 3.1 copy-start.21
  367.7 3.1 copy-start.23
  372.0 2.1 copy-start.17
  374.1 2.0 copy-start.4
  381.8 10.1 %copy-start.64 = (f32[512]{0:T(512)S(1)}, f32[512]{0:T(512)}, u32[]{:S(2)}) copy-start(f32[512]{0:T(512)} %convert_element_type.431) | copy-start | bytes 6148
  384.5 43.0 %collective-permute-start.1 = (bf16[8,512]{1,0:T(8,128)(2,1)S(1)}, bf16[8,512]{1,0:T(8,128)(2,1)S(1)}, u32[]{:S(2)}, u32[]{:S(2)}) collective-permute-start(bf16[8,512]{1,0:T(8,128)(2,1)S(1)} %get-tuple-element.35), channel_id=1, source_target_pairs={{8,0},{16,8},{24,16},{32,24},{40,32},{48,40},{56,48},{64,56},{72,6... | collective-permute-start | bytes 24584 | tf_op jit(solution)/shard_map/ppermute | solution.py:58
  386.4 41.1 %collective-permute-start = (bf16[8,512]{1,0:T(8,128)(2,1)S(1)}, bf16[8,512]{1,0:T(8,128)(2,1)S(1)}, u32[]{:S(2)}, u32[]{:S(2)}) collective-permute-start(bf16[8,512]{1,0:T(8,128)(2,1)S(1)} %get-tuple-element.34), channel_id=1, source_target_pairs={{0,8},{8,16},{16,24},{24,32},{32,40},{40,48},{48,56},{56,64},{64,7... | collective-permute-start | bytes 24584 | tf_op jit(solution)/shard_map/ppermute | solution.py:56
  436.7 4.4 copy-start.1
  (24 other events, 28.0 us)
Sparse Core Ops, SparseCore 0:
  9.2 36.0 all-gather.18
  47.1 33.3 all-gather.20
  82.3 33.3 all-gather.16
  117.4 33.3 all-gather.22
  152.5 33.3 all-gather.28
  187.5 33.3 all-gather.26
  348.3 47.0 all-gather.24
  397.2 31.7 all-gather.30
where the time goes:
time: 454 us; the launch traced here: 448 us
  blocking collectives  170 us (37%)
  matrix products  97.3 us (21%)
  local copies, waits for them, and re-layouts  78.8 us (17%)
  waiting for transfers between devices  63.8 us (14%)
  between operations  15.5 us (3%)
  other arithmetic  15 us (3%)
  starting transfers between devices  8.1 us (2%)
    all_gather x8, blocking collectives, prefix_by_axis(): lax.all_gather(part.astype(kind), axis)  130 us
    dot_general x67, matrix products, contract(): return jnp.einsum(form, left, right, precision=highest)  77.8 us
    pad x4, local copies, waits for them, and re-layouts, shards(): lax.associative_scan(chain_combine, (transfer, carried), axis=2)  50.4 us
    all_to_all x1, blocking collectives, shards(): lax.all_to_all(attn_out, 'tp', split_axis=0, concat_axis=1, tiled=True)  35.5 us
    all_gather x1, waiting for transfers between devices, shards(): lax.all_gather(value_matrix, 'fs', axis=0, tiled=True)  32.9 us
    all_gather x1, waiting for transfers between devices, shards(): lax.all_gather(key_matrix, 'fs', axis=0, tiled=True)  27.2 us
    dot_general x6, matrix products, project(): jnp.dot(left, weight, preferred_element_type=jnp.float32)  10 us
    rev x12, local copies, waits for them, and re-layouts, both_ways(): stacked = jnp.stack([forward, jnp.flip(backward, axis=0)], axis=0)  9.63 us
  transfers between devices with their start and end apart: 10, of which 2 were waited for; matrix products, arithmetic and copies ran while one was open for 40% of the time, Pallas kernels for 0%

commit v1 on v0

--- a/solution.py
+++ b/solution.py
@@ -16,6 +16,12 @@
 unit_eps = 1e-06
 span_len = 32
 highest = lax.Precision.HIGHEST
+
+
+def exchange_blocks(value, axis, split, join):
+    parts = jnp.split(value, lax.axis_size(axis), axis=split)
+    arrived = lax.all_to_all(jnp.stack(parts), axis, 0, 0)
+    return jnp.concatenate(arrived, axis=join)
 
 
 def filled_with(shard, identity):
@@ -275,7 +281,7 @@
     ]
     pool_out = jnp.concatenate(mixed, axis=1).astype(jnp.bfloat16)
     attn_half, pool_half = (
-        lax.all_to_all(attn_out, "tp", split_axis=0, concat_axis=1, tiled=True),
+        exchange_blocks(attn_out, "tp", 0, 1),
         lax.all_to_all(pool_out, "tp", split_axis=0, concat_axis=1, tiled=True),
     )
     attn_whole, pool_whole = (

time: 454 us -> 463 us (1.020)
  transfers between devices with their start and end apart: 10 -> 10, of which waited for: 2 -> 3; matrix products, arithmetic and copies ran while one was open for 40% -> 40% of each run, Pallas kernels for 0% -> 0%
where the time goes in v1:
time: 463 us; the launch traced here: 456 us
  blocking collectives  171 us (37%)
  matrix products  98 us (21%)
  local copies, waits for them, and re-layouts  81.4 us (18%)
  waiting for transfers between devices  67.3 us (15%)
  between operations  15.4 us (3%)
  other arithmetic  15.1 us (3%)
  starting transfers between devices  8.1 us (2%)
    all_gather x8, blocking collectives, prefix_by_axis(): lax.all_gather(part.astype(kind), axis)  131 us
    dot_general x67, matrix products, contract(): return jnp.einsum(form, left, right, precision=highest)  77.9 us
    pad x4, local copies, waits for them, and re-layouts, shards(): lax.associative_scan(chain_combine, (transfer, carried), axis=2)  50.3 us
    all_to_all x1, blocking collectives, exchange_blocks(): arrived = lax.all_to_all(jnp.stack(parts), axis, 0, 0)  35.6 us
    all_gather x1, waiting for transfers between devices, shards(): lax.all_gather(value_matrix, 'fs', axis=0, tiled=True)  32.9 us
    all_gather x1, waiting for transfers between devices, shards(): lax.all_gather(key_matrix, 'fs', axis=0, tiled=True)  27.2 us
    dot_general x6, matrix products, project(): jnp.dot(left, weight, preferred_element_type=jnp.float32)  10 us
    rev x12, local copies, waits for them, and re-layouts, both_ways(): stacked = jnp.stack([forward, jnp.flip(backward, axis=0)], axis=0)  9.63 us
  transfers between devices with their start and end apart: 10, of which 3 were waited for; matrix products, arithmetic and copies ran while one was open for 40% of the time, Pallas kernels for 0%

profile of v1, /device:TPU:7, one launch (start us, length us, event | category | flops | bytes accessed | tf_op | source)
XLA Modules:
  0.0 456.0 jit_solution(6429801316079691683)
XLA Ops:
  18.0 27.2 %all-gather.19.cloned.1.call-done = bf16[2048,512]{1,0:T(8,128)(2,1)} async-done(((bf16[512,512]{1,0:T(8,128)(2,1)}), bf16[2048,512]{1,0:T(8,128)(2,1)}) %all-gather.19.cloned.1.call-update) | async-done | bytes 2097168 | tf_op jit(solution)/shard_map/all_gather | solution.py:156
  45.3 2.1 fusion.29
  47.6 32.9 %all-gather.21.cloned.1.call-done = bf16[2048,512]{1,0:T(8,128)(2,1)} async-done(((bf16[512,512]{1,0:T(8,128)(2,1)}), bf16[2048,512]{1,0:T(8,128)(2,1)}) %all-gather.21.cloned.1.call-update) | async-done | bytes 2097168 | tf_op jit(solution)/shard_map/all_gather | solution.py:157
  80.5 2.1 fusion.28
  90.6 3.0 fusion.55
  93.6 3.0 convolution_select_fusion.2
  96.6 1.2 fusion.216
  97.8 1.2 fusion.217
  99.0 1.3 convolution_add_fusion.5
  100.3 1.2 fusion.218
  101.5 1.4 convolution_add_fusion.4
  102.9 2.2 fusion.219
  105.0 2.2 convolution_add_fusion.3
  107.2 4.0 convolution_select_fusion.1
  113.4 1.1 copy.129
  114.5 3.2 convolution_add_fusion.2
  117.8 1.8 convolution_negate_fusion.1
  119.6 1.2 fusion.61
  120.8 1.2 convolution_negate_fusion
  122.0 4.2 fusion.46
  126.2 5.0 %multiply_add_fusion = f32[2,8,4,64,64]{4,3,2,1,0:T(8,128)S(1)} fusion(f32[2,8,4,32,64]{4,3,2,1,0:T(8,128)S(1)} %convolution_negate_fusion.1, f32[2,8,4,64]{3,2,1,0:T(4,128)S(1)} %copy-done.55, f32[64,64]{1,0:T(8,128)S(1)} %fusion.168, f32[2,8,4,32,64]{4,1,2,3,0:T(8,128)} %copy-done.15), kind=kOutput, calls=%fused_computation.8 | convolution fusion | flops 101187584 | bytes 2129920 | tf_op jit(solution)/shard_map/...sk,...sj->...kj/dot_general | solution.py:72
  131.2 1.2 fusion.41
  133.2 4.0 convolution_add_fusion.1
  137.2 1.2 convolution_add_fusion.7
  140.2 1.5 fusion.13
  142.4 1.5 convolution_bitcast_fusion.3
  145.5 11.2 %pad.33 = f32[2,8,4,64,64]{4,3,2,1,0:T(8,128)} pad(f32[2,8,2,64,64]{4,3,2,1,0:T(8,128)S(1)} %copy-done.32, f32[]{:T(128)} %constant.27.clone.1), padding=0_0_0x0_0_0x1_0_1x0_0_0x0_0_0 | pad | bytes 1572868 | tf_op jit(solution)/shard_map/pad | solution.py:218
  156.9 11.2 %pad.32 = f32[2,8,4,64,64]{4,3,2,1,0:T(8,128)} pad(f32[2,8,2,64,64]{4,3,2,1,0:T(8,128)S(1)} %pad_maximum_fusion.1, f32[]{:T(128)} %constant.27.clone.1), padding=0_0_0x0_0_0x0_1_1x0_0_0x0_0_0 | pad | bytes 1572868 | tf_op jit(solution)/shard_map/pad | solution.py:218
  168.2 11.2 %pad.28 = f32[2,8,4,64,64]{4,3,2,1,0:T(8,128)} pad(f32[2,8,2,64,64]{4,3,2,1,0:T(8,128)S(1)} %pad_maximum_fusion, f32[]{:T(128)} %constant.27.clone.1), padding=0_0_0x0_0_0x0_1_1x0_0_0x0_0_0 | pad | bytes 1572868 | tf_op jit(solution)/shard_map/pad | solution.py:218
  179.3 16.7 %pad.29 = f32[2,8,4,64,64]{4,3,2,1,0:T(8,128)} pad(f32[2,8,2,64,64]{4,3,2,1,0:T(8,128)} %pad_add_fusion.1, f32[]{:T(128)} %constant.27.clone.1), padding=0_0_0x0_0_0x1_0_1x0_0_0x0_0_0 | pad | bytes 1572868 | tf_op jit(solution)/shard_map/pad | solution.py:218
  196.1 2.2 add_convert_fusion
  198.3 10.7 %all-gather.6 = bf16[4,8,1,64,64]{4,3,2,1,0:T(8,128)(2,1)S(1)} all-gather(bf16[1,8,1,64,64]{4,3,2,1,0:T(8,128)(2,1)S(1)} %get-tuple-element.26), channel_id=8, replica_groups=mesh['sp_0'=8,'sp_1'=4,'fs'=4,'tp'=2] {'sp_1'}, dimensions={0}, use_global_device_ids=true | all-gather | bytes 327680 | tf_op jit(solution)/shard_map/all_gather | solution.py:39
  209.0 1.8 fusion.201
  210.8 11.9 %all-gather.4 = bf16[4,8,1,64,64]{4,3,2,1,0:T(8,128)(2,1)S(1)} all-gather(bf16[1,8,1,64,64]{4,3,2,1,0:T(8,128)(2,1)S(1)} %get-tuple-element.24), channel_id=6, replica_groups=mesh['sp_0'=8,'sp_1'=4,'fs'=4,'tp'=2] {'sp_1'}, dimensions={0}, use_global_device_ids=true | all-gather | bytes 327680 | tf_op jit(solution)/shard_map/all_gather | solution.py:39
  225.5 23.0 %all-gather.7 = bf16[64,64,64]{2,1,0:T(8,128)(2,1)S(1)} all-gather(bf16[8,64,64]{2,1,0:T(8,128)(2,1)S(1)} %get-tuple-element.50), channel_id=9, replica_groups=mesh['sp_0'=8,'sp_1'=4,'fs'=4,'tp'=2] {'sp_0'}, dimensions={0}, use_global_device_ids=true | all-gather | bytes 589824 | tf_op jit(solution)/shard_map/all_gather | solution.py:39
  249.2 22.1 %all-gather.5 = bf16[64,64,64]{2,1,0:T(8,128)(2,1)S(1)} all-gather(bf16[8,64,64]{2,1,0:T(8,128)(2,1)S(1)} %get-tuple-element.52), channel_id=7, replica_groups=mesh['sp_0'=8,'sp_1'=4,'fs'=4,'tp'=2] {'sp_0'}, dimensions={0}, use_global_device_ids=true | all-gather | bytes 589824 | tf_op jit(solution)/shard_map/all_gather | solution.py:39
  273.2 10.5 %all-gather.2 = bf16[4,8,1,64,64]{4,3,2,1,0:T(8,128)(2,1)S(1)} all-gather(bf16[1,8,1,64,64]{4,3,2,1,0:T(8,128)(2,1)S(1)} %get-tuple-element.25), channel_id=4, replica_groups=mesh['sp_0'=8,'sp_1'=4,'fs'=4,'tp'=2] {'sp_1'}, dimensions={0}, use_global_device_ids=true | all-gather | bytes 327680 | tf_op jit(solution)/shard_map/all_gather | solution.py:39
  283.7 10.2 %all-gather = bf16[4,8,1,64,64]{4,3,2,1,0:T(8,128)(2,1)S(1)} all-gather(bf16[1,8,1,64,64]{4,3,2,1,0:T(8,128)(2,1)S(1)} %get-tuple-element.23), channel_id=2, replica_groups=mesh['sp_0'=8,'sp_1'=4,'fs'=4,'tp'=2] {'sp_1'}, dimensions={0}, use_global_device_ids=true | all-gather | bytes 327680 | tf_op jit(solution)/shard_map/all_gather | solution.py:39
  301.1 3.0 fusion.30
  304.1 21.9 %all-gather.3 = bf16[64,64,64]{2,1,0:T(8,128)(2,1)} all-gather(bf16[8,64,64]{2,1,0:T(8,128)(2,1)S(1)} %copy-done.53), channel_id=5, replica_groups=mesh['sp_0'=8,'sp_1'=4,'fs'=4,'tp'=2] {'sp_0'}, dimensions={0}, use_global_device_ids=true | all-gather | bytes 589824 | tf_op jit(solution)/shard_map/all_gather | solution.py:39
  326.1 1.8 copy.91
  327.8 1.9 stack.84
  329.7 1.8 rev.22
  331.5 2.0 copy.92
  333.5 2.1 copy.94
  335.6 2.0 copy.93
  338.8 1.2 fusion.214
  339.9 21.2 %all-gather.1 = bf16[64,64,64]{2,1,0:T(8,128)(2,1)S(1)} all-gather(bf16[8,64,64]{2,1,0:T(8,128)(2,1)S(1)} %get-tuple-element.56), channel_id=3, replica_groups=mesh['sp_0'=8,'sp_1'=4,'fs'=4,'tp'=2] {'sp_0'}, dimensions={0}, use_global_device_ids=true | all-gather | bytes 589824 | tf_op jit(solution)/shard_map/all_gather | solution.py:39
  365.3 1.7 fusion.16
  368.0 3.1 convolution_select_fusion.3
  371.1 1.2 fusion.222
  372.3 3.1 convolution_select_fusion
  375.4 1.2 convolution_add_fusion.6
  376.7 1.9 convolution_add_fusion.8
  378.6 2.2 convolution_bitcast_fusion
  381.3 3.4 fusion.9
  385.7 2.1 fusion.215
  387.8 1.9 collective-permute-start.1
  389.8 5.5 %collective-permute-start = (bf16[8,512]{1,0:T(8,128)(2,1)S(1)}, bf16[8,512]{1,0:T(8,128)(2,1)S(1)}, u32[]{:S(2)}, u32[]{:S(2)}) collective-permute-start(bf16[8,512]{1,0:T(8,128)(2,1)S(1)} %get-tuple-element.36), channel_id=1, source_target_pairs={{0,8},{8,16},{16,24},{24,32},{32,40},{40,48},{48,56},{56,64},{64,7... | collective-permute-start | bytes 24584 | tf_op jit(solution)/shard_map/ppermute | solution.py:62
  395.9 35.6 %all_to_all.21 = bf16[2,64,512]{2,1,0:T(8,128)(2,1)S(1)} all-to-all(bf16[2,64,512]{2,1,0:T(8,128)(2,1)S(1)} %copy.149), channel_id=1, replica_groups=mesh['sp_0'=8,'sp_1'=4,'fs'=4,'tp'=2] {'tp'}, dimensions={0} | all-to-all | bytes 262144 | tf_op jit(solution)/shard_map/all_to_all | solution.py:23
  433.2 3.8 all_to_all.22
  437.1 4.2 fusion.223
  441.2 3.4 all-gather.31.cloned.1.call-done
  444.7 4.3 fusion.1
  (302 shorter events, 49.0 us)
Async XLA Ops:
  6.5 5.0 %copy-start = (bf16[2048,128]{1,0:T(8,128)(2,1)S(1)}, bf16[2048,128]{1,0:T(8,128)(2,1)}, u32[]{:S(2)}) copy-start(bf16[2048,128]{1,0:T(8,128)(2,1)} %param.24) | copy-start | bytes 1572868
  6.5 4.7 %copy-start.64 = (f32[2,512]{1,0:T(2,128)S(1)}, f32[2,512]{1,0:T(2,128)}, u32[]{:S(2)}) copy-start(f32[2,512]{1,0:T(2,128)} %param.26) | copy-start | bytes 12292
  6.5 4.7 %copy-start.63 = (bf16[2048]{0:T(1024)(128)(2,1)S(1)}, bf16[2048]{0:T(1024)(128)(2,1)}, u32[]{:S(2)}) copy-start(bf16[2048]{0:T(1024)(128)(2,1)} %param.19) | copy-start | bytes 12292
  6.5 4.7 %copy-start.5 = (bf16[1,128,2048]{2,1,0:T(8,128)(2,1)S(1)}, bf16[1,128,2048]{2,1,0:T(8,128)(2,1)}, u32[]{:S(2)}) copy-start(bf16[1,128,2048]{2,1,0:T(8,128)(2,1)} %param.18) | copy-start | bytes 1572868
  6.5 38.7 %all-gather.19.cloned.1.call-start = ((), (), s32[]{:S(2)}) async-start(), calls=%async_computation.3 | async-start | bytes 2621440 | tf_op jit(solution)/shard_map/all_gather | solution.py:156
  7.3 73.2 %all-gather.21.cloned.1.call-start = ((), (), s32[]{:S(2)}) async-start(), calls=%async_computation.4 | async-start | bytes 2621440 | tf_op jit(solution)/shard_map/all_gather | solution.py:157
  8.0 3.9 copy-start.70
  8.0 293.1 %all-gather.17.cloned.1.call-start = ((), (), s32[]{:S(2)}) async-start(), calls=%async_computation.2 | async-start | bytes 2621440 | tf_op jit(solution)/shard_map/all_gather | solution.py:155
  8.8 356.0 %all-gather.23.cloned.1.call-start = ((), (), s32[]{:S(2)}) async-start(), calls=%async_computation.5 | async-start | bytes 2621440 | tf_op jit(solution)/shard_map/all_gather | solution.py:159
  9.3 375.9 %all-gather.27.cloned.1.call-start = ((), (), s32[]{:S(2)}) async-start(), calls=%async_computation.7 | async-start | bytes 2621440 | tf_op jit(solution)/shard_map/all_gather | solution.py:158
  9.9 2.6 copy-start.61
  9.9 2.6 copy-start.62
  10.0 385.4 %all-gather.29.cloned.1.call-start = ((), (), s32[]{:S(2)}) async-start(), calls=%async_computation.8 | async-start | bytes 2621440 | tf_op jit(solution)/shard_map/all_gather | solution.py:160
  10.5 426.6 %all-gather.25.cloned.1.call-start = ((), (), s32[]{:S(2)}) async-start(), calls=%async_computation.6 | async-start | bytes 6291456 | tf_op jit(solution)/shard_map/all_gather | solution.py:288
  11.5 69.0 %copy-start.58 = (f32[128]{0:T(128)}, f32[128]{0:T(128)S(1)}, u32[]{:S(2)}) copy-start(f32[128]{0:T(128)S(1)} %add_rsqrt_fusion.2) | copy-start | bytes 1540
  12.3 1.5 copy-start.69
  15.0 1.9 copy-start.68
  93.6 4.2 copy-start.9
  93.6 13.6 %copy-start.7 = (f32[2,8,4,32,64]{4,1,2,3,0:T(8,128)}, f32[2,8,4,32,64]{4,1,2,3,0:T(8,128)S(1)}, u32[]{:S(2)}) copy-start(f32[2,8,4,32,64]{4,1,2,3,0:T(8,128)S(1)} %get-tuple-element.14) | copy-start | bytes 1572868
  93.6 28.3 %copy-start.15 = (f32[2,8,4,32,64]{4,1,2,3,0:T(8,128)}, f32[2,8,4,32,64]{4,1,2,3,0:T(8,128)S(1)}, u32[]{:S(2)}) copy-start(f32[2,8,4,32,64]{4,1,2,3,0:T(8,128)S(1)} %get-tuple-element.18) | copy-start | bytes 1572868
  114.5 17.9 %copy-start.24 = (f32[1,4,32,8,64]{4,2,1,3,0:T(8,128)}, f32[1,4,32,8,64]{4,2,1,3,0:T(8,128)S(1)}, u32[]{:S(2)}) copy-start(f32[1,4,32,8,64]{4,2,1,3,0:T(8,128)S(1)} %copy.129) | copy-start | bytes 786436
  117.8 1.8 copy-start.22
  117.8 1.8 copy-start.30
  119.6 6.6 %copy-start.11 = (f32[2,8,4,32,64]{4,3,2,1,0:T(8,128)}, f32[2,8,4,32,64]{4,3,2,1,0:T(8,128)S(1)}, u32[]{:S(2)}) copy-start(f32[2,8,4,32,64]{4,3,2,1,0:T(8,128)S(1)} %convolution_negate_fusion.1) | copy-start | bytes 1572868
  121.9 4.2 copy-start.13
  121.9 4.2 copy-start.55
  131.2 11.2 %copy-start.2 = (f32[2,8,4,64,64]{4,3,2,1,0:T(8,128)}, f32[2,8,4,64,64]{4,3,2,1,0:T(8,128)S(1)}, u32[]{:S(2)}) copy-start(f32[2,8,4,64,64]{4,3,2,1,0:T(8,128)S(1)} %multiply_add_fusion) | copy-start | bytes 3145732
  131.2 2.0 copy-start.31
  137.2 4.5 copy-start.16
  143.9 1.6 copy-start.32
  145.5 11.2 %slice-start.1 = ((f32[2,8,4,64,64]{4,3,2,1,0:T(8,128)}), f32[2,8,1,64,64]{4,3,2,1,0:T(8,128)S(1)}, s32[]{:S(2)}) async-start(f32[2,8,4,64,64]{4,3,2,1,0:T(8,128)} %copy-done.16), calls=%async_computation.11 | async-start | bytes 1048576 | tf_op jit(solution)/shard_map/slice | solution.py:218
  145.5 11.2 %copy-start.49 = (f32[2,8,1,64,64]{4,3,2,1,0:T(8,128)S(1)}, f32[2,8,1,64,64]{4,3,2,1,0:T(8,128)}, u32[]{:S(2)}) copy-start(f32[2,8,1,64,64]{4,3,2,1,0:T(8,128)} %fusion.13) | copy-start | bytes 786436
  156.9 11.2 %slice-start = ((f32[2,8,4,64,64]{4,3,2,1,0:T(8,128)}), f32[2,8,1,64,64]{4,3,2,1,0:T(8,128)S(1)}, s32[]{:S(2)}) async-start(f32[2,8,4,64,64]{4,3,2,1,0:T(8,128)} %copy-done.2), calls=%async_computation.10 | async-start | bytes 1048576 | tf_op jit(solution)/shard_map/slice | solution.py:218
  156.9 11.2 %copy-start.50 = (f32[2,8,1,64,64]{4,3,2,1,0:T(8,128)S(1)}, f32[2,8,1,64,64]{4,3,2,1,0:T(8,128)}, u32[]{:S(2)}) copy-start(f32[2,8,1,64,64]{4,3,2,1,0:T(8,128)} %convolution_bitcast_fusion.3) | copy-start | bytes 786436
  179.3 16.7 %copy-start.3 = (f32[2,8,4,64,64]{4,3,2,1,0:T(8,128)S(1)}, f32[2,8,4,64,64]{4,3,2,1,0:T(8,128)}, u32[]{:S(2)}) copy-start(f32[2,8,4,64,64]{4,3,2,1,0:T(8,128)} %pad.33) | copy-start | bytes 3145732
  196.1 12.9 %copy-start.20 = (f32[2,8,4,64,64]{4,3,2,1,0:T(8,128)S(1)}, f32[2,8,4,64,64]{4,3,2,1,0:T(8,128)}, u32[]{:S(2)}) copy-start(f32[2,8,4,64,64]{4,3,2,1,0:T(8,128)} %pad.28) | copy-start | bytes 3145732
  196.1 12.9 %copy-start.21 = (f32[2,8,4,64,64]{4,3,2,1,0:T(8,128)S(1)}, f32[2,8,4,64,64]{4,3,2,1,0:T(8,128)}, u32[]{:S(2)}) copy-start(f32[2,8,4,64,64]{4,3,2,1,0:T(8,128)} %pad.29) | copy-start | bytes 3145732
  224.2 24.8 %copy-start.34 = (f32[8,64,64]{2,1,0:T(8,128)}, f32[8,64,64]{2,1,0:T(8,128)S(1)}, u32[]{:S(2)}) copy-start(f32[8,64,64]{2,1,0:T(8,128)S(1)} %convolution_add_fusion.19) | copy-start | bytes 393220
  224.5 24.8 %copy-start.36 = (f32[8,64,64]{2,1,0:T(8,128)}, f32[8,64,64]{2,1,0:T(8,128)S(1)}, u32[]{:S(2)}) copy-start(f32[8,64,64]{2,1,0:T(8,128)S(1)} %convolution_add_fusion.18) | copy-start | bytes 393220
  293.9 5.4 %copy-start.26 = (bf16[4,8,1,64,64]{4,3,2,1,0:T(8,128)(2,1)}, bf16[4,8,1,64,64]{4,3,2,1,0:T(8,128)(2,1)S(1)}, u32[]{:S(2)}) copy-start(bf16[4,8,1,64,64]{4,3,2,1,0:T(8,128)(2,1)S(1)} %all-gather) | copy-start | bytes 786436
  294.1 5.2 %copy-start.43 = (f32[8,64,64]{2,1,0:T(8,128)}, f32[8,64,64]{2,1,0:T(8,128)S(1)}, u32[]{:S(2)}) copy-start(f32[8,64,64]{2,1,0:T(8,128)S(1)} %fusion.130) | copy-start | bytes 393220
  299.3 1.8 copy-start.59
  301.1 3.0 copy-start.53
  333.5 4.1 copy-start.35
  333.5 4.1 copy-start.37
  333.5 4.1 copy-start.40
  333.5 4.1 copy-start.51
  333.5 4.2 copy-start.52
  333.5 5.3 %copy-start.42 = (f32[8,64,64]{2,1,0:T(8,128)S(1)}, f32[8,64,64]{2,1,0:T(8,128)}, u32[]{:S(2)}) copy-start(f32[8,64,64]{2,1,0:T(8,128)} %fusion.155) | copy-start | bytes 393220
  335.6 25.5 %copy-start.29 = (bf16[64,64,64]{2,1,0:T(8,128)(2,1)S(1)}, bf16[64,64,64]{2,1,0:T(8,128)(2,1)}, u32[]{:S(2)}) copy-start(bf16[64,64,64]{2,1,0:T(8,128)(2,1)} %all-gather.3) | copy-start | bytes 1572868
  364.8 79.9 %all-gather.31.cloned.1.call-start = ((), (), s32[]{:S(2)}) async-start(), calls=%async_computation.9 | async-start | bytes 6291456 | tf_op jit(solution)/shard_map/all_gather | solution.py:289
  365.3 2.7 copy-start.10
  365.3 2.7 copy-start.17
  365.3 2.7 copy-start.18
  368.0 3.1 copy-start.14
  372.3 3.1 copy-start.23
  372.3 3.1 copy-start.25
  376.7 1.9 copy-start.19
  376.7 1.9 copy-start.41
  378.6 2.2 copy-start.4
  387.8 7.6 %copy-start.60 = (f32[512]{0:T(512)S(1)}, f32[512]{0:T(512)}, u32[]{:S(2)}) copy-start(f32[512]{0:T(512)} %convert_element_type.430) | copy-start | bytes 6148
  387.8 43.7 %collective-permute-start.1 = (bf16[8,512]{1,0:T(8,128)(2,1)S(1)}, bf16[8,512]{1,0:T(8,128)(2,1)S(1)}, u32[]{:S(2)}, u32[]{:S(2)}) collective-permute-start(bf16[8,512]{1,0:T(8,128)(2,1)S(1)} %get-tuple-element.37), channel_id=1, source_target_pairs={{8,0},{16,8},{24,16},{32,24},{40,32},{48,40},{56,48},{64,56},{72,6... | collective-permute-start | bytes 24584 | tf_op jit(solution)/shard_map/ppermute | solution.py:64
  389.8 41.8 %collective-permute-start = (bf16[8,512]{1,0:T(8,128)(2,1)S(1)}, bf16[8,512]{1,0:T(8,128)(2,1)S(1)}, u32[]{:S(2)}, u32[]{:S(2)}) collective-permute-start(bf16[8,512]{1,0:T(8,128)(2,1)S(1)} %get-tuple-element.36), channel_id=1, source_target_pairs={{0,8},{8,16},{16,24},{24,32},{32,40},{40,48},{48,56},{56,64},{64,7... | collective-permute-start | bytes 24584 | tf_op jit(solution)/shard_map/ppermute | solution.py:62
  444.7 4.3 copy-start.1
  (20 other events, 20.2 us)
Sparse Core Ops, SparseCore 0:
  9.2 36.0 all-gather.18
  47.1 33.3 all-gather.20
  82.3 33.3 all-gather.16
  117.4 33.3 all-gather.22
  152.5 33.3 all-gather.26
  187.5 33.3 all-gather.28
  364.9 48.4 all-gather.24
  415.2 29.3 all-gather.30
